TPU v7x, 32 devices: a whole 2x2x4 slice. The times are simulated.
32 devices in a mesh: sp: 8 (over z, x), tp: 4 (over y, core).
Axes of the slice: x: 2, y: 2, z: 4, core: 2. Of those that a mesh axis runs over, the one named last changes fastest.
Arguments:
- x_res: bfloat16 [2048, 2048], P(('sp', 'tp')), may hold values from -6 to 6
- q_a: bfloat16 [2048, 1024], P('sp', 'tp'), may hold values from -48 to 48
- k_a: bfloat16 [2048, 256], P('sp', 'tp'), may hold values from -48 to 48
- v_a: bfloat16 [2048, 256], P('sp', 'tp'), may hold values from -6 to 6
- q_b: bfloat16 [2048, 1024], P('sp', 'tp'), may hold values from -48 to 48
- k_b: bfloat16 [2048, 512], P('sp', 'tp'), may hold values from -48 to 48
- v_b: bfloat16 [2048, 512], P('sp', 'tp'), may hold values from -6 to 6
- gain_qa: float32 [64], replicated, may hold values from 1.2 to 6
- gain_ka: float32 [64], replicated, may hold values from 1.2 to 6
- gain_qb: float32 [128], replicated, may hold values from 1.2 to 6
- gain_kb: float32 [128], replicated, may hold values from 1.2 to 6
- w_out_a: bfloat16 [1024, 2048], P('tp'), may hold values from -0.125 to 0.125
- w_out_b: bfloat16 [1024, 2048], P('tp'), may hold values from -0.125 to 0.125
- gain_mid: float32 [2048], replicated, may hold values from 0.1 to 1.9
- w_gate: bfloat16 [2048, 3072], P('sp', 'tp'), may hold values from -0.125 to 0.125
- w_up: bfloat16 [2048, 3072], P('sp', 'tp'), may hold values from -0.125 to 0.125
- conv_gate: float32 [3, 3072], P(None, 'tp'), may hold values from -3.5 to 3.5
- conv_up: float32 [3, 3072], P(None, 'tp'), may hold values from -3.5 to 3.5
- w_down: bfloat16 [3072, 2048], P('tp', 'sp'), may hold values from -0.109375 to 0.109375
Outputs:
- layer_out: bfloat16 [2048, 2048], P(('sp', 'tp'))
All inputs are finite; a program needn't handle non-finite values.
Results may differ from a plain program's by a relative error of at most 0.014.
The roundings to bfloat16 on the way count: a program that leaves them out, or rounds other values in their place, can miss the bound.
Values may be sent and summed in bfloat16 or wider, within the bound.
A program may use at most 128 MiB of HBM per device.

v0:
```python
import jax
import jax.numpy as jnp
from jax import lax
from jax.sharding import PartitionSpec as P

DHA = 64
DHB = 128


norm_eps = 1e-06
rope_theta = 10000.0


def extended(block, sides, width):
    for axis, dim in sides:
        count = lax.axis_size(axis)
        forward = [(i, i + 1) for i in range(count - 1)]
        backward = [(target, source) for source, target in forward]
        low = lax.ppermute(
            lax.slice_in_dim(block, block.shape[dim] - width, None, axis=dim), axis, forward
        )
        high = lax.ppermute(lax.slice_in_dim(block, 0, width, axis=dim), axis, backward)
        block = jnp.concatenate([low, block, high], axis=dim)
    return block


def rotary_angles(positions, head_size):
    half = head_size // 2
    inverse = jnp.power(jnp.float32(rope_theta), -jnp.arange(0, half, 2, dtype=jnp.float32) / half)
    grid_row = (positions // 64).astype(jnp.float32)[:, None] * inverse[None, :]
    grid_col = (positions % 64).astype(jnp.float32)[:, None] * inverse[None, :]
    angles = jnp.concatenate([grid_row, grid_row, grid_col, grid_col], axis=-1)
    return (jnp.cos(angles), jnp.sin(angles))


def rotate_half(values):
    first, second = jnp.split(values, 2, axis=-1)
    return jnp.concatenate([-second, first], axis=-1)


def prepare(raw, gain, head_size, positions):
    count = raw.shape[0]
    heads = raw.shape[1] // head_size
    values = raw.astype(jnp.float32).reshape(count, heads, head_size)
    values = values * lax.rsqrt(jnp.mean(values * values, axis=-1, keepdims=True) + norm_eps)
    values = values * gain
    cosine, sine = rotary_angles(positions, head_size)
    row_part, col_part = jnp.split(values, 2, axis=-1)
    turned = jnp.concatenate([rotate_half(row_part), rotate_half(col_part)], axis=-1)
    values = values * cosine[:, None, :] + turned * sine[:, None, :]
    return values.astype(jnp.bfloat16)


def start_state(queries):
    count, kv_heads, groups, head_size = queries.shape
    lowest = jnp.full((kv_heads, groups, count), -1e30, jnp.float32)
    totals = jnp.zeros((kv_heads, groups, count), jnp.float32)
    summed = jnp.zeros((kv_heads, groups, count, head_size), jnp.float32)
    return (lowest, totals, summed)


def attend(state, queries, key_piece, value_piece):
    head_size = queries.shape[3]
    kv_heads = queries.shape[1]
    length = key_piece.shape[0]
    keys = key_piece.reshape(length, kv_heads, head_size)
    values = value_piece.reshape(length, kv_heads, head_size)
    span = length
    while span > 1024 and span % 2 == 0:
        span = span // 2
    scale = jnp.float32(head_size ** (-0.5))

    def one_span(index, carry):
        running, totals, summed = carry
        key_rows = lax.dynamic_slice_in_dim(keys, index * span, span, 0)
        value_rows = lax.dynamic_slice_in_dim(values, index * span, span, 0)
        scores = (
            jnp.einsum("qkgd,skd->kgqs", queries, key_rows, preferred_element_type=jnp.float32)
            * scale
        )
        highest = jnp.maximum(running, jnp.max(scores, axis=-1))
        factor = jnp.exp(running - highest)
        expd = jnp.exp(scores - highest[..., None])
        totals = totals * factor + jnp.sum(expd, axis=-1)
        summed = summed * factor[..., None] + jnp.einsum(
            "kgqs,skd->kgqd",
            expd.astype(jnp.bfloat16),
            value_rows,
            preferred_element_type=jnp.float32,
        )
        return (highest, totals, summed)

    return lax.fori_loop(0, length // span, one_span, state)


def finish(state):
    running, totals, summed = state
    kv_heads, groups, count, head_size = summed.shape
    result = summed / totals[..., None]
    return (
        jnp.transpose(result, (2, 0, 1, 3))
        .reshape(count, kv_heads * groups * head_size)
        .astype(jnp.bfloat16)
    )


def on_device(
    x_res,
    q_a,
    k_a,
    v_a,
    q_b,
    k_b,
    v_b,
    gain_qa,
    gain_ka,
    gain_qb,
    gain_kb,
    w_out_a,
    w_out_b,
    gain_mid,
    w_gate,
    w_up,
    conv_gate,
    conv_up,
    w_down,
):
    tok_rows = q_a.shape[0]
    whole_gate, whole_up, whole_down = (
        lax.all_gather(w_gate, "sp", axis=0, tiled=True),
        lax.all_gather(w_up, "sp", axis=0, tiled=True),
        lax.all_gather(w_down, "sp", axis=1, tiled=True),
    )
    positions = lax.axis_index("sp") * tok_rows + lax.iota(jnp.int32, tok_rows)
    kv_a = k_a.shape[1] // DHA
    kv_b = k_b.shape[1] // DHB
    query_a = prepare(q_a, gain_qa, DHA, positions)
    query_a = query_a.reshape(tok_rows, kv_a, query_a.shape[1] // kv_a, DHA)
    query_b = prepare(q_b, gain_qb, DHB, positions)
    query_b = query_b.reshape(tok_rows, kv_b, query_b.shape[1] // kv_b, DHB)
    keys_a = prepare(k_a, gain_ka, DHA, positions).reshape(tok_rows, kv_a * DHA)
    keys_b = prepare(k_b, gain_kb, DHB, positions).reshape(tok_rows, kv_b * DHB)
    state_a = attend(
        start_state(query_a),
        query_a,
        lax.all_gather(keys_a, "sp", axis=0, tiled=True),
        lax.all_gather(v_a, "sp", axis=0, tiled=True),
    )
    state_b = attend(
        start_state(query_b),
        query_b,
        lax.all_gather(keys_b, "sp", axis=0, tiled=True),
        lax.all_gather(v_b, "sp", axis=0, tiled=True),
    )
    attn_a = finish(state_a)
    attn_b = finish(state_b)
    projected = lax.psum_scatter(
        (
            jnp.dot(attn_a, w_out_a, preferred_element_type=jnp.float32)
            + jnp.dot(attn_b, w_out_b, preferred_element_type=jnp.float32)
        ).astype(jnp.bfloat16),
        "tp",
        scatter_dimension=0,
        tiled=True,
    ).astype(jnp.float32)
    middle = x_res.astype(jnp.float32) + projected
    normed = middle * lax.rsqrt(jnp.mean(middle * middle, axis=-1, keepdims=True) + norm_eps)
    normed = (normed * gain_mid).astype(jnp.bfloat16)
    gathered = lax.all_gather(normed, "tp", axis=0, tiled=True)
    gate_pre = jnp.dot(gathered, whole_gate, preferred_element_type=jnp.float32)
    up_pre = jnp.dot(gathered, whole_up, preferred_element_type=jnp.float32)
    width = gate_pre.shape[1]
    joined = jnp.concatenate([gate_pre, up_pre], axis=1).astype(jnp.bfloat16)
    padded = extended(joined, (("sp", 0),), 1)
    taps = jnp.concatenate([conv_gate, conv_up], axis=1)
    mixed = padded[:-2] * taps[0] + padded[1:-1] * taps[1] + padded[2:] * taps[2]
    hidden = (jax.nn.silu(mixed[:, :width]) * mixed[:, width:]).astype(jnp.bfloat16)
    terms = jnp.dot(hidden, whole_down, preferred_element_type=jnp.float32)
    summed = lax.psum_scatter(
        terms.astype(jnp.bfloat16), "tp", scatter_dimension=0, tiled=True
    ).astype(jnp.float32)
    return (middle + summed).astype(jnp.bfloat16)


def solution(mesh):
    in_specs = (
        P(("sp", "tp"), None),
        P("sp", "tp"),
        P("sp", "tp"),
        P("sp", "tp"),
        P("sp", "tp"),
        P("sp", "tp"),
        P("sp", "tp"),
        P(),
        P(),
        P(),
        P(),
        P("tp", None),
        P("tp", None),
        P(),
        P("sp", "tp"),
        P("sp", "tp"),
        P(None, "tp"),
        P(None, "tp"),
        P("tp", "sp"),
    )
    out_specs = P(("sp", "tp"), None)
    return jax.shard_map(
        on_device, mesh=mesh, in_specs=in_specs, out_specs=out_specs, check_vma=False
    )
```

profile of v0, /device:TPU:0, one launch (start us, length us, event | category | flops | bytes accessed | tf_op | source)
XLA Modules:
  0.0 438.9 jit_solution(5774465157238761757)
XLA Ops:
  6.6 0.6 multiply_power_fusion.1
  7.2 1.0 fusion.48
  8.2 0.9 fusion.50
  9.4 1.5 fusion.53
  11.7 35.5 %all_gather.26 = bf16[2048,128]{1,0:T(8,128)(2,1)} all-gather(bf16[256,128]{1,0:T(8,128)(2,1)S(1)} %get-tuple-element.349), channel_id=1, replica_groups=mesh['sp'=8,'tp'=4] {'sp'}, dimensions={0}, use_global_device_ids=true | all-gather | bytes 589824 | tf_op jit(solution)/shard_map/all_gather | solution.py:152
  47.2 33.4 %all_gather.27 = bf16[2048,128]{1,0:T(8,128)(2,1)} all-gather(bf16[256,128]{1,0:T(8,128)(2,1)S(1)} %copy-done.11), channel_id=1, replica_groups=mesh['sp'=8,'tp'=4] {'sp'}, dimensions={0}, use_global_device_ids=true | all-gather | bytes 589824 | tf_op jit(solution)/shard_map/all_gather | solution.py:153
  80.6 7.8 %while.37 = (s32[]{:T(128)}, f32[1,2,256]{2,1,0:T(2,128)S(1)}, f32[1,2,256]{2,1,0:T(2,128)}, f32[1,2,256,128]{3,2,1,0:T(8,128)S(1)}, bf16[2048,1,128]{2,0,1:T(8,...) while((s32[]{:T(128)}, f32[1,2,256]{2,1,0:T(2,128)S(1)}, ...), condition=%wide.region_11.12_spmd.clone, body=%wide.region_8.11_spmd.clone.sunk | while | flops 272829440 | bytes 7520487 | solution.py:93
  80.6 1.4 bitcast_reduce_fusion.5
  82.0 1.5 fusion.109
  83.9 0.6 copy-done.9
  84.5 1.4 bitcast_reduce_fusion.5
  85.9 1.5 fusion.109
  87.8 0.6 copy-done.9
  88.5 0.7 broadcast_multiply_fusion.3
  89.3 0.8 fusion.56
  90.1 0.8 fusion.58
  90.9 1.0 copy.26
  92.0 0.7 multiply_multiply_fusion.1
  92.9 30.7 %all_gather.24 = bf16[2048,64]{0,1:T(8,128)(2,1)S(1)} all-gather(bf16[256,64]{0,1:T(8,128)(2,1)S(1)} %get-tuple-element.375), channel_id=1, replica_groups=mesh['sp'=8,'tp'=4] {'sp'}, dimensions={0}, use_global_device_ids=true | all-gather | bytes 294912 | tf_op jit(solution)/shard_map/all_gather | solution.py:146
  123.7 30.7 %all_gather.25 = bf16[2048,64]{0,1:T(8,128)(2,1)S(1)} all-gather(bf16[256,64]{0,1:T(8,128)(2,1)S(1)} %copy-done.12), channel_id=1, replica_groups=mesh['sp'=8,'tp'=4] {'sp'}, dimensions={0}, use_global_device_ids=true | all-gather | bytes 294912 | tf_op jit(solution)/shard_map/all_gather | solution.py:147
  154.5 13.8 %while.36 = (s32[]{:T(128)}, f32[1,4,256]{2,1,0:T(4,128)S(1)}, f32[1,4,256]{2,1,0:T(4,128)S(1)}, f32[1,4,256,64]{2,3,1,0:T(8,128)S(1)}, bf16[2048,1,64]{0,2,1:T(...) while((s32[]{:T(128)}, f32[1,4,256]{2,1,0:T(4,128)S(1)}, ...), condition=%wide.region_5.6_spmd.clone, body=%wide.region_2.5_spmd.clone.sunk | while | flops 277026816 | bytes 30343368 | solution.py:93
  154.6 2.7 bitcast_reduce_fusion.4
  157.3 3.2 fusion.104
  160.7 0.7 fusion.103
  161.5 2.7 bitcast_reduce_fusion.4
  164.2 3.2 fusion.104
  167.6 0.7 fusion.103
  168.9 0.7 copy-done.5
  169.6 1.4 fusion.40
  171.1 26.1 %reduce-scatter.3.cloned.1.call-done = bf16[64,2048]{1,0:T(8,128)(2,1)} async-done(((bf16[256,2048]{1,0:T(8,128)(2,1)}), bf16[64,2048]{1,0:T(8,128)(2,1)}) %reduce-scatter.3.cloned.1.call-update) | async-done | bytes 262160 | tf_op jit(solution)/shard_map/reduce_scatter | solution.py:157
  197.2 1.1 multiply_reduce_fusion
  198.4 1.8 multiply_convert_fusion
  200.2 0.7 all-gather.9.cloned.1.call-update
  201.0 0.5 all-gather.7.cloned.1.call-update
  201.5 0.5 all-gather.11.cloned.1.call-update
  202.2 14.9 %all-gather.5.cloned.1.call-done = bf16[256,2048]{1,0:T(8,128)(2,1)} async-done(((bf16[64,2048]{1,0:T(8,128)(2,1)}), bf16[256,2048]{1,0:T(8,128)(2,1)}) %all-gather.5.cloned.1.call-update) | async-done | bytes 1048592 | tf_op jit(solution)/shard_map/all_gather | solution.py:169
  217.0 62.2 %all-gather.9.cloned.1.call-done = bf16[2048,768]{1,0:T(8,128)(2,1)} async-done(((bf16[256,768]{1,0:T(8,128)(2,1)}), bf16[2048,768]{1,0:T(8,128)(2,1)}) %all-gather.9.cloned.1.call-update) | async-done | bytes 3145744 | tf_op jit(solution)/shard_map/all_gather | solution.py:131
  279.3 3.2 convolution_convert_fusion.1
  282.5 57.6 %all-gather.7.cloned.1.call-done = bf16[2048,768]{1,0:T(8,128)(2,1)} async-done(((bf16[256,768]{1,0:T(8,128)(2,1)}), bf16[2048,768]{1,0:T(8,128)(2,1)}) %all-gather.7.cloned.1.call-update) | async-done | bytes 3145744 | tf_op jit(solution)/shard_map/all_gather | solution.py:130
  340.0 2.9 convolution_convert_fusion.2
  342.9 2.5 collective-permute-start
  345.4 1.3 collective-permute-start.1
  346.8 4.6 %collective-permute-done.1 = bf16[1,1536]{1,0:T(2,128)(2,1)S(1)} collective-permute-done((bf16[1,1536]{1,0:T(2,128)(2,1)S(1)}, bf16[1,1536]{1,0:T(2,128)(2,1)S(1)}, u32[]{:S(2)}, u32[]{:S(2)}) %collective-permute-start.1) | collective-permute-done | bytes 3104 | tf_op jit(solution)/shard_map/ppermute | solution.py:22
  351.3 0.5 multiply_add_fusion
  351.9 51.4 %all-gather.11.cloned.1.call-done = bf16[768,2048]{1,0:T(8,128)(2,1)} async-done(((bf16[768,256]{1,0:T(8,128)(2,1)}), bf16[768,2048]{1,0:T(8,128)(2,1)}) %all-gather.11.cloned.1.call-update) | async-done | bytes 3145744 | tf_op jit(solution)/shard_map/all_gather | solution.py:132
  403.3 3.9 convolution_convert_fusion
  407.2 23.1 %reduce-scatter.5.cloned.1.call-done = bf16[64,2048]{1,0:T(8,128)(2,1)} async-done(((bf16[256,2048]{1,0:T(8,128)(2,1)}), bf16[64,2048]{1,0:T(8,128)(2,1)}) %reduce-scatter.5.cloned.1.call-update) | async-done | bytes 262160 | tf_op jit(solution)/shard_map/reduce_scatter | solution.py:179
  430.3 1.7 add_convert_fusion
  (107 shorter events, 3.7 us)
Async XLA Ops:
  6.5 161.9 %copy-start = (bf16[256,2048]{1,0:T(8,128)(2,1)S(1)}, bf16[256,2048]{1,0:T(8,128)(2,1)}, u32[]{:S(2)}) copy-start(bf16[256,2048]{1,0:T(8,128)(2,1)} %param.34) | copy-start | bytes 3145732
  6.5 4.6 %copy-start.7 = (bf16[256,256]{1,0:T(8,128)(2,1)S(1)}, bf16[256,256]{1,0:T(8,128)(2,1)}, u32[]{:S(2)}) copy-start(bf16[256,256]{1,0:T(8,128)(2,1)} %param.27) | copy-start | bytes 393220
  6.5 4.8 %copy-start.19 = (f32[128]{0:T(128)S(1)}, f32[128]{0:T(128)}, u32[]{:S(2)}) copy-start(f32[128]{0:T(128)} %param.32) | copy-start | bytes 1540
  6.5 190.7 %reduce-scatter.3.cloned.1.call-start = ((), (), s32[]{:S(2)}) async-start(), calls=%async_computation.2 | async-start | bytes 1310720 | tf_op jit(solution)/shard_map/reduce_scatter | solution.py:157
  7.2 2.2 copy-start.15
  7.2 2.2 copy-start.16
  9.4 37.7 %copy-start.11 = (bf16[256,128]{1,0:T(8,128)(2,1)S(1)}, bf16[256,128]{1,0:T(8,128)(2,1)}, u32[]{:S(2)}) copy-start(bf16[256,128]{1,0:T(8,128)(2,1)} %param.29) | copy-start | bytes 196612
  82.0 1.9 copy-start.8
  83.9 0.6 copy-start.9
  85.9 1.9 copy-start.8
  87.8 0.6 copy-start.9
  88.4 4.4 %copy-start.6 = (bf16[256,64]{0,1:T(8,128)(2,1)S(1)}, bf16[256,64]{0,1:T(8,128)(2,1)}, u32[]{:S(2)}) copy-start(bf16[256,64]{0,1:T(8,128)(2,1)} %param.25) | copy-start | bytes 98308
  88.4 4.4 %copy-start.18 = (f32[64]{0:T(128)S(1)}, f32[64]{0:T(128)}, u32[]{:S(2)}) copy-start(f32[64]{0:T(128)} %param.31) | copy-start | bytes 772
  88.4 35.3 %copy-start.12 = (bf16[256,64]{0,1:T(8,128)(2,1)S(1)}, bf16[256,64]{0,1:T(8,128)(2,1)}, u32[]{:S(2)}) copy-start(bf16[256,64]{0,1:T(8,128)(2,1)} %param.26) | copy-start | bytes 98308
  88.4 66.0 %copy-start.20 = (f32[64]{0:T(128)S(1)}, f32[64]{0:T(128)}, u32[]{:S(2)}) copy-start(f32[64]{0:T(128)} %param.30) | copy-start | bytes 772
  88.4 66.1 %copy-start.2 = (f32[1,4,256,64]{2,3,1,0:T(8,128)S(1)}, f32[1,4,256,64]{2,3,1,0:T(8,128)}, u32[]{:S(2)}) copy-start(f32[1,4,256,64]{2,3,1,0:T(8,128)} %custom-call.2) | copy-start | bytes 786436
  154.5 13.9 %copy-start.10 = (f32[1,2,256]{2,1,0:T(2,128)S(1)}, f32[1,2,256]{2,1,0:T(2,128)}, u32[]{:S(2)}) copy-start(f32[1,2,256]{2,1,0:T(2,128)} %get-tuple-element.258) | copy-start | bytes 6148
  157.3 3.5 copy-start.1
  164.2 3.5 copy-start.1
  168.4 1.2 copy-start.5
  169.6 27.6 %copy-start.3 = (bf16[64,2048]{1,0:T(8,128)(2,1)S(1)}, bf16[64,2048]{1,0:T(8,128)(2,1)}, u32[]{:S(2)}) copy-start(bf16[64,2048]{1,0:T(8,128)(2,1)} %param.23) | copy-start | bytes 786436
  169.6 28.8 %copy-start.17 = (f32[2048]{0:T(1024)S(1)}, f32[2048]{0:T(1024)}, u32[]{:S(2)}) copy-start(f32[2048]{0:T(1024)} %param.36) | copy-start | bytes 24580
  171.0 31.1 %copy-start.13 = (f32[3,768]{1,0:T(4,128)S(1)}, f32[3,768]{1,0:T(4,128)}, u32[]{:S(2)}) copy-start(f32[3,768]{1,0:T(4,128)} %param.39) | copy-start | bytes 27652
  171.0 31.1 %copy-start.14 = (f32[3,768]{1,0:T(4,128)S(1)}, f32[3,768]{1,0:T(4,128)}, u32[]{:S(2)}) copy-start(f32[3,768]{1,0:T(4,128)} %param.40) | copy-start | bytes 27652
  171.1 46.0 %all-gather.5.cloned.1.call-start = ((), (), s32[]{:S(2)}) async-start(), calls=%async_computation.3 | async-start | bytes 1310720 | tf_op jit(solution)/shard_map/all_gather | solution.py:169
  200.2 79.1 %all-gather.9.cloned.1.call-start = ((), (), s32[]{:S(2)}) async-start(), calls=%async_computation.5 | async-start | bytes 3538944 | tf_op jit(solution)/shard_map/all_gather | solution.py:131
  200.9 139.1 %all-gather.7.cloned.1.call-start = ((), (), s32[]{:S(2)}) async-start(), calls=%async_computation.4 | async-start | bytes 3538944 | tf_op jit(solution)/shard_map/all_gather | solution.py:130
  201.5 201.8 %all-gather.11.cloned.1.call-start = ((), (), s32[]{:S(2)}) async-start(), calls=%async_computation.6 | async-start | bytes 3538944 | tf_op jit(solution)/shard_map/all_gather | solution.py:132
  202.1 228.3 %reduce-scatter.5.cloned.1.call-start = ((), (), s32[]{:S(2)}) async-start(), calls=%async_computation.7 | async-start | bytes 1310720 | tf_op jit(solution)/shard_map/reduce_scatter | solution.py:179
  217.0 123.0 %copy-start.21 = (bf16[256,2048]{1,0:T(8,128)(2,1)S(1)}, bf16[256,2048]{1,0:T(8,128)(2,1)}, u32[]{:S(2)}) copy-start(bf16[256,2048]{1,0:T(8,128)(2,1)} %all-gather.5.cloned.1.call-done) | copy-start | bytes 3145732
  342.9 3.8 collective-permute-start
  345.4 5.9 %collective-permute-start.1 = (bf16[1,1536]{1,0:T(2,128)(2,1)S(1)}, bf16[1,1536]{1,0:T(2,128)(2,1)S(1)}, u32[]{:S(2)}, u32[]{:S(2)}) collective-permute-start(bf16[1,1536]{1,0:T(2,128)(2,1)S(1)} %get-tuple-element.357), channel_id=1, source_target_pairs={{4,0},{8,4},{12,8},{16,12},{20,16},{24,20},{28,24},{5,1},{9,5},{13... | collective-permute-start | bytes 9224 | tf_op jit(solution)/shard_map/ppermute | solution.py:22
  351.9 78.5 %copy-start.4 = (bf16[64,2048]{1,0:T(8,128)(2,1)S(1)}, bf16[64,2048]{1,0:T(8,128)(2,1)}, u32[]{:S(2)}) copy-start(bf16[64,2048]{1,0:T(8,128)(2,1)} %reduce-scatter.3.cloned.1.call-done) | copy-start | bytes 786436
Sparse Core Ops, SparseCore 0:
  171.2 25.9 reduce-scatter.2
  200.3 16.6 all-gather.4
  219.2 59.9 all-gather.8
  281.3 58.6 all-gather.6
  341.9 61.3 all-gather.10
  407.3 22.9 reduce-scatter.4
where the time goes:
time: 440 us; the launch traced here: 439 us
  waiting for transfers between devices  242 us (55%)
  blocking collectives  130 us (30%)
  matrix products  29.5 us (7%)
  other arithmetic  15.5 us (4%)
  between operations  13.9 us (3%)
    all_gather x1, waiting for transfers between devices, on_device(): lax.all_gather(w_up, 'sp', axis=0, tiled=True)  62.2 us
    all_gather x1, waiting for transfers between devices, on_device(): lax.all_gather(w_gate, 'sp', axis=0, tiled=True)  57.6 us
    all_gather x1, waiting for transfers between devices, on_device(): lax.all_gather(w_down, 'sp', axis=1, tiled=True)  51.4 us
    all_gather x1, blocking collectives, on_device(): lax.all_gather(keys_b, 'sp', axis=0, tiled=True)  35.5 us
    all_gather x1, blocking collectives, on_device(): lax.all_gather(v_b, 'sp', axis=0, tiled=True)  33.4 us
    all_gather x1, blocking collectives, on_device(): lax.all_gather(keys_a, 'sp', axis=0, tiled=True)  30.7 us
    all_gather x1, blocking collectives, on_device(): lax.all_gather(v_a, 'sp', axis=0, tiled=True)  30.7 us
    reduce_scatter x1, waiting for transfers between devices, on_device(): lax.psum_scatter((jnp.dot(attn_a, w_out_a, preferred_element_type=jnp.flo...  26.1 us
  transfers between devices with their start and end apart: 8, of which 7 were waited for; matrix products, arithmetic and copies ran while one was open for 2% of the time, Pallas kernels for 0%

commit v1 on v0

--- a/solution.py
+++ b/solution.py
@@ -1,14 +1,525 @@
+import functools
+
 import jax
 import jax.numpy as jnp
 from jax import lax
+from jax.experimental import pallas as pl
+from jax.experimental.pallas import tpu as pltpu
 from jax.sharding import PartitionSpec as P
 
 DHA = 64
 DHB = 128
 
-
 norm_eps = 1e-06
 rope_theta = 10000.0
+F32 = jnp.float32
+BF16 = jnp.bfloat16
+MESH = pl.DeviceIdType.MESH
+PIECES = 2
+
+
+def rotary_angles(positions, head_size):
+    half = head_size // 2
+    inverse = jnp.power(jnp.float32(rope_theta), -jnp.arange(0, half, 2, dtype=jnp.float32) / half)
+    grid_row = (positions // 64).astype(jnp.float32)[:, None] * inverse[None, :]
+    grid_col = (positions % 64).astype(jnp.float32)[:, None] * inverse[None, :]
+    return jnp.concatenate([grid_row, grid_row, grid_col, grid_col], axis=-1)
+
+
+def block_mean(width, head):
+    i = lax.broadcasted_iota(jnp.int32, (width, width), 0)
+    j = lax.broadcasted_iota(jnp.int32, (width, width), 1)
+    return jnp.where(lax.div(i, head) == lax.div(j, head), F32(1.0 / head), F32(0.0))
+
+
+def block_turn(width, head):
+    quarter = head // 4
+    i = lax.broadcasted_iota(jnp.int32, (width, width), 0)
+    j = lax.broadcasted_iota(jnp.int32, (width, width), 1)
+    first = lax.rem(j, 2 * quarter) < quarter
+    return jnp.where(
+        first & (i == j + quarter),
+        F32(-1.0),
+        jnp.where(jnp.logical_not(first) & (i == j - quarter), F32(1.0), F32(0.0)),
+    )
+
+
+def exact_dot(a, b):
+    return jnp.dot(a, b, precision=lax.Precision.HIGHEST, preferred_element_type=F32)
+
+
+def prepared(raw, gain, angle_cos, angle_sin, head):
+    width = raw.shape[1]
+    values = raw.astype(F32)
+    values = values * lax.rsqrt(exact_dot(values * values, block_mean(width, head)) + norm_eps)
+    values = values * gain
+    turned = exact_dot(values, block_turn(width, head))
+    return (values * angle_cos + turned * angle_sin).astype(BF16)
+
+
+def kernel(
+    n, tp_n,
+    x_ref, qa_ref, ka_ref, va_ref, qb_ref, kb_ref, vb_ref,
+    gqa_ref, gka_ref, gqb_ref, gkb_ref,
+    cosa_ref, sina_ref, cosb_ref, sinb_ref,
+    woa_hbm, wob_hbm, gmid_ref, wg_hbm, wu_hbm, cg_ref, cu_ref, wd_hbm,
+    out_ref,
+    kv, qas, qbs, m_a, l_a, acc_a, m_b, l_b, acc_b,
+    woa, wob, wg, wu, wdr, wdl,
+    attn, part, rs_in, mid, nrm, acc_g, acc_u, joined, halo_lo, halo_hi, hidden, acc_d, part2, rs2_in,
+    loc_sem, kv_send, kv_recv, w_send, w_recv, d_send, d_recv,
+    rs_send, rs_recv, ag_send, ag_recv, h_send, h_recv, r2_send, r2_recv,
+):
+    sp = lax.axis_index("sp")
+    tp = lax.axis_index("tp")
+    rows = qa_ref.shape[0]
+    own = x_ref.shape[0]
+    half = n // 2
+
+    odd = lax.rem(sp, 2)
+    pos = (1 - odd) * lax.div(sp, 2) + odd * (n - 1 - lax.div(sp, 2))
+
+    def at(p):
+        p = lax.rem(p + 2 * n, n)
+        back = lax.div(p, half)
+        return (1 - back) * 2 * p + back * (2 * (n - 1 - p) + 1)
+
+    right, left = at(pos + 1), at(pos - 1)
+    above, below = lax.rem(sp + 1, n), lax.rem(sp + n - 1, n)
+
+    barrier = pltpu.get_barrier_semaphore()
+    for other in (right, left, above, below):
+        pl.semaphore_signal(barrier, inc=1, device_id={"sp": other}, device_id_type=MESH)
+    for d in range(1, tp_n):
+        pl.semaphore_signal(
+            barrier, inc=1, device_id={"tp": lax.rem(tp + d, tp_n)}, device_id_type=MESH
+        )
+
+    locals_ = [
+        pltpu.make_async_copy(woa_hbm, woa, loc_sem.at[0]),
+        pltpu.make_async_copy(wob_hbm, wob, loc_sem.at[1]),
+        pltpu.make_async_copy(wg_hbm, wg.at[0], loc_sem.at[2]),
+        pltpu.make_async_copy(wu_hbm, wu.at[0], loc_sem.at[3]),
+        pltpu.make_async_copy(wd_hbm.at[pl.ds(0, wdr.shape[1])], wdr.at[0], loc_sem.at[4]),
+        pltpu.make_async_copy(
+            wd_hbm.at[pl.ds(wdr.shape[1], wdr.shape[1])], wdl.at[0], loc_sem.at[5]
+        ),
+    ]
+    for copy in locals_:
+        copy.start()
+
+    def remote(src, dst, send, recv, **where):
+        return pltpu.make_async_remote_copy(
+            src_ref=src, dst_ref=dst, send_sem=send, recv_sem=recv,
+            device_id=where, device_id_type=MESH,
+        )
+
+    ca, sa, cb, sb = cosa_ref[...], sina_ref[...], cosb_ref[...], sinb_ref[...]
+    wka, wkb = ka_ref.shape[1], kb_ref.shape[1]
+
+    def wide(table, width):
+        if width <= table.shape[1]:
+            return table[:, :width]
+        return jnp.concatenate([table] * (width // table.shape[1]), axis=1)
+
+    def gains(ref, width):
+        g = ref[...]
+        count = width // g.shape[1]
+        return g if count == 1 else jnp.concatenate([g] * count, axis=1)
+
+    keys_a = prepared(ka_ref[...], gains(gka_ref, wka), wide(ca, wka), wide(sa, wka), DHA)
+    keys_b = prepared(kb_ref[...], gains(gkb_ref, wkb), wide(cb, wkb), wide(sb, wkb), DHB)
+    kv[0, :, :wkb] = keys_b
+    kv[0, :, wkb:2 * wkb] = vb_ref[...]
+    kv[0, :, 2 * wkb:] = jnp.concatenate([keys_a, va_ref[...]], axis=1)
+    pl.semaphore_wait(barrier, 4 + tp_n - 1)
+
+    def kv_r(s):
+        return remote(kv.at[s - 1], kv.at[s], kv_send.at[s], kv_recv.at[s], sp=right)
+
+    def kv_l(s):
+        source = lax.rem(n - s + 1, n)
+        return remote(kv.at[source], kv.at[n - s], kv_send.at[n - s], kv_recv.at[n - s], sp=left)
+
+    wrows = wg.shape[1] // PIECES
+    drows = wdr.shape[1] // PIECES
+
+    def w_copy(s, p, direction):
+        buf, to = (wg, right) if direction == 0 else (wu, left)
+        cut = pl.ds(p * wrows, wrows)
+        return remote(
+            buf.at[s - 1, cut], buf.at[s, cut],
+            w_send.at[direction, p, s], w_recv.at[direction, p, s], sp=to,
+        )
+
+    def d_copy(s, p, direction):
+        buf, to = (wdr, right) if direction == 0 else (wdl, left)
+        cut = pl.ds(p * drows, drows)
+        return remote(
+            buf.at[s - 1, cut], buf.at[s, cut],
+            d_send.at[direction, p, s], d_recv.at[direction, p, s], sp=to,
+        )
+
+    def tick(copy, s, following=None):
+        for p in range(PIECES):
+            for direction in range(2):
+                copy(s, p, direction).wait_recv()
+                if following is None:
+                    copy(s + 1, p, direction).start()
+                elif following != "end":
+                    following(1, p, direction).start()
+
+    kv_r(1).start()
+    kv_l(1).start()
+
+    heads_a = qa_ref.shape[1] // DHA
+    heads_b = qb_ref.shape[1] // DHB
+    qa = prepared(
+        qa_ref[...], gains(gqa_ref, heads_a * DHA), wide(ca, heads_a * DHA),
+        wide(sa, heads_a * DHA), DHA,
+    )
+    qb = prepared(
+        qb_ref[...], gains(gqb_ref, heads_b * DHB), wide(cb, heads_b * DHB),
+        wide(sb, heads_b * DHB), DHB,
+    )
+    for h in range(heads_a):
+        qas[h] = qa[:, h * DHA:(h + 1) * DHA]
+    for h in range(heads_b):
+        qbs[h] = qb[:, h * DHB:(h + 1) * DHB]
+    for ref, low in ((m_a, -1e30), (m_b, -1e30), (l_a, 0.0), (l_b, 0.0), (acc_a, 0.0), (acc_b, 0.0)):
+        ref[...] = jnp.full(ref.shape, low, F32)
+
+    def attend_one(queries, key_rows, value_rows, m, l, acc, h):
+        scale = F32(queries.shape[2] ** (-0.5))
+        scores = lax.dot_general(
+            queries[h], key_rows, (((1,), (1,)), ((), ())), preferred_element_type=F32
+        ) * scale
+        before = m[h]
+        highest = jnp.maximum(before, jnp.max(scores, axis=-1, keepdims=True))
+        factor = jnp.exp(before - highest)
+        expd = jnp.exp(scores - highest)
+        l[h] = l[h] * factor + jnp.sum(expd, axis=-1, keepdims=True)
+        acc[h] = acc[h] * factor + jnp.dot(
+            expd.astype(BF16), value_rows, preferred_element_type=F32
+        )
+        m[h] = highest
+
+    def attend(slot):
+        for h in range(heads_b):
+            attend_one(qbs, kv[slot, :, :wkb], kv[slot, :, wkb:2 * wkb], m_b, l_b, acc_b, h)
+        pair = kv[slot, :, 2 * wkb:]
+        for h in range(heads_a):
+            attend_one(qas, pair[:, :wka], pair[:, wka:], m_a, l_a, acc_a, h)
+
+    attend(0)
+
+    def kv_step(s, carry):
+        kv_r(s).wait_recv()
+        kv_r(s + 1).start()
+        kv_l(s).wait_recv()
+
+        @pl.when(s < half - 1)
+        def _():
+            kv_l(s + 1).start()
+
+        @pl.when(s == half - 1)
+        def _():
+            for p in range(PIECES):
+                for direction in range(2):
+                    w_copy(1, p, direction).start()
+
+        def one(i, inner):
+            attend((1 - i) * s + i * (n - s))
+            return inner
+
+        lax.fori_loop(0, 2, one, 0)
+        return carry
+
+    for copy in locals_:
+        copy.wait()
+    lax.fori_loop(1, half, kv_step, 0)
+    kv_r(half).wait_recv()
+    attend(half)
+
+    for h in range(heads_a):
+        attn[:, h * DHA:(h + 1) * DHA] = (acc_a[h] / l_a[h]).astype(BF16)
+    width_a = heads_a * DHA
+    for h in range(heads_b):
+        attn[:, width_a + h * DHB:width_a + (h + 1) * DHB] = (acc_b[h] / l_b[h]).astype(BF16)
+
+    def rs_copy(d):
+        to = lax.rem(tp + d, tp_n)
+        return remote(
+            part.at[pl.ds(pl.multiple_of(to * own, own), own)], rs_in.at[d - 1],
+            rs_send.at[d - 1], rs_recv.at[d - 1], tp=to,
+        )
+
+    for i in range(tp_n):
+        d = tp_n - 1 - i
+        at_rows = pl.ds(pl.multiple_of(lax.rem(tp + d, tp_n) * own, own), own)
+        block = attn[at_rows, :]
+        part[at_rows, :] = (
+            jnp.dot(block[:, :width_a], woa[...], preferred_element_type=F32)
+            + jnp.dot(block[:, width_a:], wob[...], preferred_element_type=F32)
+        ).astype(BF16)
+        if d > 0:
+            rs_copy(d).start()
+
+    early = max(1, n // 8)
+
+    def w_tick(s, carry):
+        tick(w_copy, s)
+        return carry
+
+    lax.fori_loop(1, early + 1, w_tick, 0)
+
+    mine = pl.ds(pl.multiple_of(tp * own, own), own)
+    total = part[mine, :].astype(F32)
+    for d in range(1, tp_n):
+        rs_copy(d).wait_recv()
+        total = total + rs_in[d - 1].astype(F32)
+    middle = x_ref[...].astype(F32) + total
+    mid[...] = middle
+    normed = middle * lax.rsqrt(jnp.mean(middle * middle, axis=-1, keepdims=True) + norm_eps)
+    nrm[mine, :] = (normed * gmid_ref[...]).astype(BF16)
+
+    def ag_copy(d):
+        return remote(
+            nrm.at[mine], nrm.at[mine], ag_send.at[d - 1], ag_recv.at[d - 1],
+            tp=lax.rem(tp + d, tp_n),
+        )
+
+    for d in range(1, tp_n):
+        ag_copy(d).start()
+    lax.fori_loop(early + 1, 2 * early + 1, w_tick, 0)
+    for d in range(1, tp_n):
+        ag_copy(d).wait_recv()
+
+    chunk = wg.shape[1]
+
+    def columns(p, width):
+        return pl.ds(pl.multiple_of(at(p) * width, width), width)
+
+    def gate_up(s):
+        acc_g[...] += jnp.dot(nrm[:, columns(pos - s, chunk)], wg[s], preferred_element_type=F32)
+        acc_u[...] += jnp.dot(nrm[:, columns(pos + s, chunk)], wu[s], preferred_element_type=F32)
+
+    acc_g[...] = jnp.zeros_like(acc_g)
+    acc_u[...] = jnp.zeros_like(acc_u)
+
+    def w_caught_up(s, carry):
+        gate_up(s)
+        return carry
+
+    def w_step(s, carry):
+        tick(w_copy, s)
+        gate_up(s)
+        return carry
+
+    lax.fori_loop(0, 2 * early + 1, w_caught_up, 0)
+    lax.fori_loop(2 * early + 1, n - 1, w_step, 0)
+    tick(w_copy, n - 1, following=d_copy)
+    gate_up(n - 1)
+
+    width = acc_g.shape[1]
+    joined[:, :width] = acc_g[...].astype(BF16)
+    joined[:, width:] = acc_u[...].astype(BF16)
+    edge = halo_lo.shape[0]
+    up_copy = remote(
+        joined.at[pl.ds(rows - edge, edge)], halo_lo, h_send.at[0], h_recv.at[0], sp=above
+    )
+    down_copy = remote(joined.at[pl.ds(0, edge)], halo_hi, h_send.at[1], h_recv.at[1], sp=below)
+    up_copy.start()
+    down_copy.start()
+
+    def d_tick(s, carry):
+        tick(d_copy, s)
+        return carry
+
+    lax.fori_loop(1, 2, d_tick, 0)
+    up_copy.wait_recv()
+    down_copy.wait_recv()
+    has_low = jnp.where(sp > 0, F32(1.0), F32(0.0))
+    has_high = jnp.where(sp < n - 1, F32(1.0), F32(0.0))
+
+    def convolved(start, taps_ref):
+        cut = slice(start, start + width)
+        now = joined[:, cut].astype(F32)
+        low = halo_lo[:, cut].astype(F32)[edge - 1:edge] * has_low
+        high = halo_hi[:, cut].astype(F32)[0:1] * has_high
+        line = lax.broadcasted_iota(jnp.int32, now.shape, 0)
+        before = jnp.where(line == 0, low, pltpu.roll(now, 1, 0))
+        after = jnp.where(line == rows - 1, high, pltpu.roll(now, rows - 1, 0))
+        taps = taps_ref[...]
+        return before * taps[0:1] + now * taps[1:2] + after * taps[2:3]
+
+    gate = convolved(0, cg_ref)
+    up = convolved(width, cu_ref)
+    hidden[...] = (gate / (1.0 + jnp.exp(-gate)) * up).astype(BF16)
+
+    dcols = wdr.shape[2]
+    split = wdr.shape[1]
+    acc_d[...] = jnp.zeros_like(acc_d)
+
+    def down(s):
+        acc_d[at(pos - s)] += jnp.dot(hidden[:, :split], wdr[s], preferred_element_type=F32)
+        acc_d[at(pos + s)] += jnp.dot(hidden[:, split:], wdl[s], preferred_element_type=F32)
+
+    def r2_copy(r, d):
+        block = at(pos - r)
+        to = lax.rem(tp + d, tp_n)
+        return remote(
+            part2.at[block, pl.ds(pl.multiple_of(to * own, own), own)], rs2_in.at[d - 1, block],
+            r2_send.at[r, d - 1], r2_recv.at[r, d - 1], tp=to,
+        )
+
+    def give(r):
+        block = at(pos - r)
+        part2[block] = acc_d[block].astype(BF16)
+        for d in range(1, tp_n):
+            r2_copy(r, d).start()
+
+    def d_caught_up(s, carry):
+        down(s)
+        return carry
+
+    def d_step(s, carry):
+        tick(d_copy, s)
+        down(s)
+        return carry
+
+    def d_step_give(s, carry):
+        tick(d_copy, s)
+        down(s)
+        give(s)
+        give(n - s)
+        return carry
+
+    lax.fori_loop(0, 2, d_caught_up, 0)
+    lax.fori_loop(2, half, d_step, 0)
+    give(0)
+    tick(d_copy, half)
+    down(half)
+    give(half)
+    lax.fori_loop(half + 1, n - 1, d_step_give, 0)
+    tick(d_copy, n - 1, following="end")
+    down(n - 1)
+    give(n - 1)
+    give(1)
+
+    def sent_r(s, carry):
+        kv_r(s).wait_send()
+        return carry
+
+    def sent_l(s, carry):
+        kv_l(s).wait_send()
+        return carry
+
+    def sent_w(s, carry):
+        for p in range(PIECES):
+            for direction in range(2):
+                w_copy(s, p, direction).wait_send()
+                d_copy(s, p, direction).wait_send()
+        return carry
+
+    lax.fori_loop(1, half + 1, sent_r, 0)
+    lax.fori_loop(1, half, sent_l, 0)
+    lax.fori_loop(1, n, sent_w, 0)
+    up_copy.wait_send()
+    down_copy.wait_send()
+    for d in range(1, tp_n):
+        rs_copy(d).wait_send()
+        ag_copy(d).wait_send()
+
+    def arrived(r, carry):
+        for d in range(1, tp_n):
+            r2_copy(r, d).wait_send()
+            r2_copy(r, d).wait_recv()
+        return carry
+
+    lax.fori_loop(0, n, arrived, 0)
+    for block in range(n):
+        cut = slice(block * dcols, (block + 1) * dcols)
+        summed = part2[block, mine].astype(F32)
+        for d in range(1, tp_n):
+            summed = summed + rs2_in[d - 1, block].astype(F32)
+        out_ref[:, cut] = (mid[:, cut] + summed).astype(out_ref.dtype)
+
+
+def on_device(n, tp_n, *args):
+    if n % 2 or n < 8 or args[14].shape[0] % 128 or args[18].shape[1] % 128:
+        return on_device_narrow(*args)
+    (x_res, q_a, k_a, v_a, q_b, k_b, v_b, gain_qa, gain_ka, gain_qb, gain_kb, w_out_a, w_out_b,
+     gain_mid, w_gate, w_up, conv_gate, conv_up, w_down) = args
+    rows = q_a.shape[0]
+    own, width = x_res.shape
+    ff = w_gate.shape[1]
+    heads_a, heads_b = q_a.shape[1] // DHA, q_b.shape[1] // DHB
+    positions = lax.axis_index("sp") * rows + lax.iota(jnp.int32, rows)
+    angle_a = rotary_angles(positions, DHA)
+    angle_a = jnp.concatenate([angle_a, angle_a], axis=1)
+    angle_b = rotary_angles(positions, DHB)
+    cos_a, sin_a, cos_b, sin_b = jnp.cos(angle_a), jnp.sin(angle_a), jnp.cos(angle_b), jnp.sin(angle_b)
+    vmem = pl.BlockSpec(memory_space=pltpu.VMEM)
+    hbm = pl.BlockSpec(memory_space=pltpu.MemorySpace.HBM)
+    edge = 16
+    kv_width = 2 * k_a.shape[1] + 2 * k_b.shape[1]
+    dma = pltpu.SemaphoreType.DMA
+    scratch = [
+        pltpu.VMEM((n, rows, kv_width), BF16),
+        pltpu.VMEM((heads_a, rows, DHA), BF16),
+        pltpu.VMEM((heads_b, rows, DHB), BF16),
+        pltpu.VMEM((heads_a, rows, 1), F32),
+        pltpu.VMEM((heads_a, rows, 1), F32),
+        pltpu.VMEM((heads_a, rows, DHA), F32),
+        pltpu.VMEM((heads_b, rows, 1), F32),
+        pltpu.VMEM((heads_b, rows, 1), F32),
+        pltpu.VMEM((heads_b, rows, DHB), F32),
+        pltpu.VMEM(w_out_a.shape, BF16),
+        pltpu.VMEM(w_out_b.shape, BF16),
+        pltpu.VMEM((n,) + w_gate.shape, BF16),
+        pltpu.VMEM((n,) + w_up.shape, BF16),
+        pltpu.VMEM((n, ff // 2, w_down.shape[1]), BF16),
+        pltpu.VMEM((n, ff // 2, w_down.shape[1]), BF16),
+        pltpu.VMEM((rows, q_a.shape[1] + q_b.shape[1]), BF16),
+        pltpu.VMEM((rows, width), BF16),
+        pltpu.VMEM((tp_n - 1, own, width), BF16),
+        pltpu.VMEM((own, width), F32),
+        pltpu.VMEM((rows, width), BF16),
+        pltpu.VMEM((rows, ff), F32),
+        pltpu.VMEM((rows, ff), F32),
+        pltpu.VMEM((rows, 2 * ff), BF16),
+        pltpu.VMEM((edge, 2 * ff), BF16),
+        pltpu.VMEM((edge, 2 * ff), BF16),
+        pltpu.VMEM((rows, ff), BF16),
+        pltpu.VMEM((n, rows, w_down.shape[1]), F32),
+        pltpu.VMEM((n, rows, w_down.shape[1]), BF16),
+        pltpu.VMEM((tp_n - 1, n, own, w_down.shape[1]), BF16),
+        dma((6,)),
+        dma((n,)), dma((n,)),
+        dma((2, PIECES, n)), dma((2, PIECES, n)),
+        dma((2, PIECES, n)), dma((2, PIECES, n)),
+        dma((tp_n - 1,)), dma((tp_n - 1,)),
+        dma((tp_n - 1,)), dma((tp_n - 1,)),
+        dma((2,)), dma((2,)),
+        dma((n, tp_n - 1)), dma((n, tp_n - 1)),
+    ]
+    return pl.pallas_call(
+        functools.partial(kernel, n, tp_n),
+        out_shape=jax.ShapeDtypeStruct(x_res.shape, BF16),
+        in_specs=[vmem] * 15 + [hbm, hbm, vmem, hbm, hbm, vmem, vmem, hbm],
+        out_specs=vmem,
+        scratch_shapes=scratch,
+        compiler_params=pltpu.CompilerParams(
+            collective_id=0, has_side_effects=True, vmem_limit_bytes=60 * 1024 * 1024
+        ),
+        name="layer",
+    )(
+        x_res, q_a, k_a, v_a, q_b, k_b, v_b,
+        gain_qa[None], gain_ka[None], gain_qb[None], gain_kb[None],
+        cos_a, sin_a, cos_b, sin_b,
+        w_out_a, w_out_b, gain_mid[None], w_gate, w_up, conv_gate, conv_up, w_down,
+    )
 
 
 def extended(block, sides, width):
@@ -24,15 +535,6 @@
     return block
 
 
-def rotary_angles(positions, head_size):
-    half = head_size // 2
-    inverse = jnp.power(jnp.float32(rope_theta), -jnp.arange(0, half, 2, dtype=jnp.float32) / half)
-    grid_row = (positions // 64).astype(jnp.float32)[:, None] * inverse[None, :]
-    grid_col = (positions % 64).astype(jnp.float32)[:, None] * inverse[None, :]
-    angles = jnp.concatenate([grid_row, grid_row, grid_col, grid_col], axis=-1)
-    return (jnp.cos(angles), jnp.sin(angles))
-
-
 def rotate_half(values):
     first, second = jnp.split(values, 2, axis=-1)
     return jnp.concatenate([-second, first], axis=-1)
@@ -44,7 +546,8 @@
     values = raw.astype(jnp.float32).reshape(count, heads, head_size)
     values = values * lax.rsqrt(jnp.mean(values * values, axis=-1, keepdims=True) + norm_eps)
     values = values * gain
-    cosine, sine = rotary_angles(positions, head_size)
+    angles = rotary_angles(positions, head_size)
+    cosine, sine = jnp.cos(angles), jnp.sin(angles)
     row_part, col_part = jnp.split(values, 2, axis=-1)
     turned = jnp.concatenate([rotate_half(row_part), rotate_half(col_part)], axis=-1)
     values = values * cosine[:, None, :] + turned * sine[:, None, :]
@@ -104,7 +607,7 @@
     )
 
 
-def on_device(
+def on_device_narrow(
     x_res,
     q_a,
     k_a,
@@ -205,6 +708,7 @@
         P("tp", "sp"),
     )
     out_specs = P(("sp", "tp"), None)
+    body = functools.partial(on_device, mesh.shape["sp"], mesh.shape["tp"])
     return jax.shard_map(
-        on_device, mesh=mesh, in_specs=in_specs, out_specs=out_specs, check_vma=False
-    )
+        body, mesh=mesh, in_specs=in_specs, out_specs=out_specs, check_vma=False
+    )

time: 440 us -> 138 us (0.31)
  waiting for transfers between devices: 242 us -> 0 us
  Pallas kernels: 0 us -> 131 us
  blocking collectives: 130 us -> 0 us
  matrix products: 29.5 us -> 0 us
  other arithmetic: 15.5 us -> 1.56 us
  between operations: 13.9 us -> 0.05 us
    all_gather x4 -> x0, waiting for transfers between devices: 186 us -> none  [the longest x1 62.2 us: on_device(): lax.all_gather(w_up, 'sp', axis=0, tiled=True)]
    pallas_call x0 -> x1, Pallas kernels: none -> 131 us  [on_device(): pl.pallas_call(functools.partial(kernel, n, tp_n), out_shape=jax.ShapeDty...]
    all_gather x4 -> x0, blocking collectives: 130 us -> none  [the longest x1 35.5 us: on_device(): lax.all_gather(keys_b, 'sp', axis=0, tiled=True)]
    reduce_scatter x2 -> x0, waiting for transfers between devices: 49.2 us -> none  [the longest x1 26.1 us: on_device(): lax.psum_scatter((jnp.dot(attn_a, w_out_a, preferred_element_type=jnp.flo...]
    dot_general x13 -> x0, matrix products: 29.5 us -> none  [the longest x4 9.41 us: one_span(): jnp.einsum('kgqs,skd->kgqd', expd.astype(jnp.bfloat16), value_rows, prefe...]
    convert_element_type x7 -> x0, other arithmetic: 5.29 us -> none  [the longest x1 1.77 us: on_device(): normed = (normed * gain_mid).astype(jnp.bfloat16)]
    reduce_sum x9 -> x0, other arithmetic: 5.07 us -> none  [the longest x4 2.12 us: one_span(): totals = totals * factor + jnp.sum(expd, axis=-1)]
    ppermute x2 -> x0, waiting for transfers between devices: 4.56 us -> none  [the longest x1 4.56 us: extended(): lax.ppermute(lax.slice_in_dim(block, 0, width, axis=dim), axis, backward)]
  transfers between devices with their start and end apart: 8 -> 0, of which waited for: 7 -> 0; matrix products, arithmetic and copies ran while one was open for 2% -> 0% of each run, Pallas kernels for 0% -> 0%
where the time goes in v1:
time: 138 us
  Pallas kernels  131 us (95%)
  local copies, waits for them, and re-layouts  5.35 us (4%)
  other arithmetic  1.56 us (1%)
    pallas_call x1, Pallas kernels, on_device(): pl.pallas_call(functools.partial(kernel, n, tp_n), out_shape=jax.ShapeDty...  131 us
    unnamed x5, local copies, waits for them, and re-layouts  3.88 us

profile of v1, /device:TPU:0, one launch (start us, length us, event | category | flops | bytes accessed | tf_op | source)
XLA Modules:
  0.0 137.6 jit_solution(8919074318035657631)
XLA Ops:
  0.0 0.0 copy-start
  0.1 1.5 %copy.20.ka_ref = bf16[256,64]{1,0:T(8,128)(2,1)} copy(bf16[256,64]{0,1:T(8,128)(2,1)} %param.21) | data formatting | bytes 65536 | tf_op args[2]
  1.5 0.0 copy-done
  1.5 0.7 copy.21.va_ref
  2.3 0.1 broadcast_multiply_fusion.1
  2.4 1.3 fusion
  3.7 0.1 broadcast_multiply_fusion.2
  3.8 0.3 concatenate.8
  4.1 1.2 fusion.5
  5.3 130.6 %layer.1 = bf16[64,2048]{1,0:T(8,128)(2,1)} custom-call(bf16[64,2048]{1,0:T(8,128)(2,1)} %x_ref.1, bf16[256,256]{1,0:T(8,128)(2,1)} %qa_ref.1, bf16[256,64]{1,0:T(8,128)(2,1)} %copy.20.ka_ref, bf16[256,64]{1,0:T(8,128)(2,1)} %copy.21.va_ref, bf16[256,256]{1,0:T(8,128)(2,1)} %qb_ref.1, bf16[256,128]{1,0:T(8,128)(2,1)} %kb_ref.1, bf16[256,128]{1,0:T(8,128)(2,1)} %vb_ref.1, ...), custom_call_target="tpu_custom_call" | custom-call | tf_op jit(solution)/shard_map/layer/pallas_call | solution.py:507
  135.9 1.7 %copy.23 = bf16[64,2048]{1,0:T(8,128)(2,1)} copy(bf16[64,2048]{1,0:T(8,128)(2,1)} %layer.1) | data formatting | bytes 524288
  (3 shorter events, 0.0 us)
Async XLA Ops:
  0.0 1.5 %copy-start = (bf16[256,64]{0,1:T(8,128)(2,1)S(1)}, bf16[256,64]{0,1:T(8,128)(2,1)}, u32[]{:S(2)}) copy-start(bf16[256,64]{0,1:T(8,128)(2,1)} %param.22) | copy-start | bytes 98308

commit v2 on v1

--- a/solution.py
+++ b/solution.py
@@ -15,7 +15,7 @@
 F32 = jnp.float32
 BF16 = jnp.bfloat16
 MESH = pl.DeviceIdType.MESH
-PIECES = 2
+PIECES = 4
 
 
 def rotary_angles(positions, head_size):
@@ -24,6 +24,12 @@
     grid_row = (positions // 64).astype(jnp.float32)[:, None] * inverse[None, :]
     grid_col = (positions % 64).astype(jnp.float32)[:, None] * inverse[None, :]
     return jnp.concatenate([grid_row, grid_row, grid_col, grid_col], axis=-1)
+
+
+def lane_frequencies(head_size, width):
+    half = head_size // 2
+    inverse = jnp.power(jnp.float32(rope_theta), -jnp.arange(0, half, 2, dtype=jnp.float32) / half)
+    return jnp.tile(inverse, width // inverse.shape[0])[None]
 
 
 def block_mean(width, head):
@@ -59,12 +65,12 @@
 
 def kernel(
     n, tp_n,
-    x_ref, qa_ref, ka_ref, va_ref, qb_ref, kb_ref, vb_ref,
+    x_ref, qa_ref, ka_hbm, va_hbm, qb_ref, kb_ref, vb_ref,
     gqa_ref, gka_ref, gqb_ref, gkb_ref,
-    cosa_ref, sina_ref, cosb_ref, sinb_ref,
+    fra_ref, frb_ref,
     woa_hbm, wob_hbm, gmid_ref, wg_hbm, wu_hbm, cg_ref, cu_ref, wd_hbm,
     out_ref,
-    kv, qas, qbs, m_a, l_a, acc_a, m_b, l_b, acc_b,
+    ka_ref, va_ref, kv, qas, qbs, m_a, l_a, acc_a, m_b, l_b, acc_b,
     woa, wob, wg, wu, wdr, wdl,
     attn, part, rs_in, mid, nrm, acc_g, acc_u, joined, halo_lo, halo_hi, hidden, acc_d, part2, rs2_in,
     loc_sem, kv_send, kv_recv, w_send, w_recv, d_send, d_recv,
@@ -105,7 +111,11 @@
             wd_hbm.at[pl.ds(wdr.shape[1], wdr.shape[1])], wdl.at[0], loc_sem.at[5]
         ),
     ]
-    for copy in locals_:
+    small = [
+        pltpu.make_async_copy(ka_hbm, ka_ref, loc_sem.at[6]),
+        pltpu.make_async_copy(va_hbm, va_ref, loc_sem.at[7]),
+    ]
+    for copy in locals_[2:4] + small + locals_[4:] + locals_[:2]:
         copy.start()
 
     def remote(src, dst, send, recv, **where):
@@ -113,26 +123,6 @@
             src_ref=src, dst_ref=dst, send_sem=send, recv_sem=recv,
             device_id=where, device_id_type=MESH,
         )
-
-    ca, sa, cb, sb = cosa_ref[...], sina_ref[...], cosb_ref[...], sinb_ref[...]
-    wka, wkb = ka_ref.shape[1], kb_ref.shape[1]
-
-    def wide(table, width):
-        if width <= table.shape[1]:
-            return table[:, :width]
-        return jnp.concatenate([table] * (width // table.shape[1]), axis=1)
-
-    def gains(ref, width):
-        g = ref[...]
-        count = width // g.shape[1]
-        return g if count == 1 else jnp.concatenate([g] * count, axis=1)
-
-    keys_a = prepared(ka_ref[...], gains(gka_ref, wka), wide(ca, wka), wide(sa, wka), DHA)
-    keys_b = prepared(kb_ref[...], gains(gkb_ref, wkb), wide(cb, wkb), wide(sb, wkb), DHB)
-    kv[0, :, :wkb] = keys_b
-    kv[0, :, wkb:2 * wkb] = vb_ref[...]
-    kv[0, :, 2 * wkb:] = jnp.concatenate([keys_a, va_ref[...]], axis=1)
-    pl.semaphore_wait(barrier, 4 + tp_n - 1)
 
     def kv_r(s):
         return remote(kv.at[s - 1], kv.at[s], kv_send.at[s], kv_recv.at[s], sp=right)
@@ -167,7 +157,54 @@
                 if following is None:
                     copy(s + 1, p, direction).start()
                 elif following != "end":
-                    following(1, p, direction).start()
+                    following(1, p, direction).wait_recv()
+                    following(2, p, direction).start()
+
+    def begin(copy, s, low, high):
+        for p in range(low, high):
+            for direction in range(2):
+                copy(s, p, direction).start()
+
+    def pass_on(copy, s, low, high):
+        for p in range(low, high):
+            for direction in range(2):
+                copy(s, p, direction).wait_recv()
+                copy(s + 1, p, direction).start()
+
+    pl.semaphore_wait(barrier, 4 + tp_n - 1)
+    for copy in locals_[2:4]:
+        copy.wait()
+    begin(w_copy, 1, 0, PIECES // 2)
+
+    def tables(freq_ref, head):
+        shape = (rows, freq_ref.shape[1])
+        token = lax.broadcasted_iota(jnp.int32, shape, 0) + sp * rows
+        lane = lax.broadcasted_iota(jnp.int32, shape, 1)
+        grid = jnp.where(lax.rem(lane, head) < head // 2, lax.div(token, 64), lax.rem(token, 64))
+        angles = grid.astype(F32) * freq_ref[...]
+        return jnp.cos(angles), jnp.sin(angles)
+
+    ca, sa = tables(fra_ref, DHA)
+    cb, sb = tables(frb_ref, DHB)
+    for copy in small:
+        copy.wait()
+    wka, wkb = ka_ref.shape[1], kb_ref.shape[1]
+
+    def wide(table, width):
+        if width <= table.shape[1]:
+            return table[:, :width]
+        return jnp.concatenate([table] * (width // table.shape[1]), axis=1)
+
+    def gains(ref, width):
+        g = ref[...]
+        count = width // g.shape[1]
+        return g if count == 1 else jnp.concatenate([g] * count, axis=1)
+
+    keys_a = prepared(ka_ref[...], gains(gka_ref, wka), wide(ca, wka), wide(sa, wka), DHA)
+    keys_b = prepared(kb_ref[...], gains(gkb_ref, wkb), wide(cb, wkb), wide(sb, wkb), DHB)
+    kv[0, :, :wkb] = keys_b
+    kv[0, :, wkb:2 * wkb] = vb_ref[...]
+    kv[0, :, 2 * wkb:] = jnp.concatenate([keys_a, va_ref[...]], axis=1)
 
     kv_r(1).start()
     kv_l(1).start()
@@ -222,11 +259,17 @@
         def _():
             kv_l(s + 1).start()
 
-        @pl.when(s == half - 1)
+        @pl.when(s == 1)
         def _():
-            for p in range(PIECES):
-                for direction in range(2):
-                    w_copy(1, p, direction).start()
+            begin(w_copy, 1, PIECES // 2, PIECES)
+
+        @pl.when(s == 2)
+        def _():
+            begin(d_copy, 1, 0, PIECES)
+
+        @pl.when(s == 3)
+        def _():
+            pass_on(w_copy, 1, 0, PIECES // 2)
 
         def one(i, inner):
             attend((1 - i) * s + i * (n - s))
@@ -235,10 +278,11 @@
         lax.fori_loop(0, 2, one, 0)
         return carry
 
-    for copy in locals_:
+    for copy in locals_[:2] + locals_[4:]:
         copy.wait()
     lax.fori_loop(1, half, kv_step, 0)
     kv_r(half).wait_recv()
+    pass_on(w_copy, 1, PIECES // 2, PIECES)
     attend(half)
 
     for h in range(heads_a):
@@ -265,13 +309,11 @@
         if d > 0:
             rs_copy(d).start()
 
-    early = max(1, n // 8)
-
     def w_tick(s, carry):
         tick(w_copy, s)
         return carry
 
-    lax.fori_loop(1, early + 1, w_tick, 0)
+    lax.fori_loop(2, 4, w_tick, 0)
 
     mine = pl.ds(pl.multiple_of(tp * own, own), own)
     total = part[mine, :].astype(F32)
@@ -291,7 +333,7 @@
 
     for d in range(1, tp_n):
         ag_copy(d).start()
-    lax.fori_loop(early + 1, 2 * early + 1, w_tick, 0)
+    lax.fori_loop(4, 6, w_tick, 0)
     for d in range(1, tp_n):
         ag_copy(d).wait_recv()
 
@@ -316,8 +358,9 @@
         gate_up(s)
         return carry
 
-    lax.fori_loop(0, 2 * early + 1, w_caught_up, 0)
-    lax.fori_loop(2 * early + 1, n - 1, w_step, 0)
+    lax.fori_loop(0, 4, w_caught_up, 0)
+    lax.fori_loop(6, n - 1, w_step, 0)
+    lax.fori_loop(4, 6, w_caught_up, 0)
     tick(w_copy, n - 1, following=d_copy)
     gate_up(n - 1)
 
@@ -332,11 +375,7 @@
     up_copy.start()
     down_copy.start()
 
-    def d_tick(s, carry):
-        tick(d_copy, s)
-        return carry
-
-    lax.fori_loop(1, 2, d_tick, 0)
+    tick(d_copy, 2)
     up_copy.wait_recv()
     down_copy.wait_recv()
     has_low = jnp.where(sp > 0, F32(1.0), F32(0.0))
@@ -354,8 +393,9 @@
         return before * taps[0:1] + now * taps[1:2] + after * taps[2:3]
 
     gate = convolved(0, cg_ref)
-    up = convolved(width, cu_ref)
-    hidden[...] = (gate / (1.0 + jnp.exp(-gate)) * up).astype(BF16)
+    acc_g[...] = gate / (1.0 + jnp.exp(-gate))
+    tick(d_copy, 3)
+    hidden[...] = (acc_g[...] * convolved(width, cu_ref)).astype(BF16)
 
     dcols = wdr.shape[2]
     split = wdr.shape[1]
@@ -395,8 +435,8 @@
         give(n - s)
         return carry
 
-    lax.fori_loop(0, 2, d_caught_up, 0)
-    lax.fori_loop(2, half, d_step, 0)
+    lax.fori_loop(0, 4, d_caught_up, 0)
+    lax.fori_loop(4, half, d_step, 0)
     give(0)
     tick(d_copy, half)
     down(half)
@@ -455,17 +495,15 @@
     own, width = x_res.shape
     ff = w_gate.shape[1]
     heads_a, heads_b = q_a.shape[1] // DHA, q_b.shape[1] // DHB
-    positions = lax.axis_index("sp") * rows + lax.iota(jnp.int32, rows)
-    angle_a = rotary_angles(positions, DHA)
-    angle_a = jnp.concatenate([angle_a, angle_a], axis=1)
-    angle_b = rotary_angles(positions, DHB)
-    cos_a, sin_a, cos_b, sin_b = jnp.cos(angle_a), jnp.sin(angle_a), jnp.cos(angle_b), jnp.sin(angle_b)
+    freq_a, freq_b = lane_frequencies(DHA, 2 * DHA), lane_frequencies(DHB, DHB)
     vmem = pl.BlockSpec(memory_space=pltpu.VMEM)
     hbm = pl.BlockSpec(memory_space=pltpu.MemorySpace.HBM)
     edge = 16
     kv_width = 2 * k_a.shape[1] + 2 * k_b.shape[1]
     dma = pltpu.SemaphoreType.DMA
     scratch = [
+        pltpu.VMEM(k_a.shape, BF16),
+        pltpu.VMEM(v_a.shape, BF16),
         pltpu.VMEM((n, rows, kv_width), BF16),
         pltpu.VMEM((heads_a, rows, DHA), BF16),
         pltpu.VMEM((heads_b, rows, DHB), BF16),
@@ -495,7 +533,7 @@
         pltpu.VMEM((n, rows, w_down.shape[1]), F32),
         pltpu.VMEM((n, rows, w_down.shape[1]), BF16),
         pltpu.VMEM((tp_n - 1, n, own, w_down.shape[1]), BF16),
-        dma((6,)),
+        dma((8,)),
         dma((n,)), dma((n,)),
         dma((2, PIECES, n)), dma((2, PIECES, n)),
         dma((2, PIECES, n)), dma((2, PIECES, n)),
@@ -507,7 +545,7 @@
     return pl.pallas_call(
         functools.partial(kernel, n, tp_n),
         out_shape=jax.ShapeDtypeStruct(x_res.shape, BF16),
-        in_specs=[vmem] * 15 + [hbm, hbm, vmem, hbm, hbm, vmem, vmem, hbm],
+        in_specs=[vmem] * 2 + [hbm] * 2 + [vmem] * 9 + [hbm, hbm, vmem, hbm, hbm, vmem, vmem, hbm],
         out_specs=vmem,
         scratch_shapes=scratch,
         compiler_params=pltpu.CompilerParams(
@@ -517,7 +555,7 @@
     )(
         x_res, q_a, k_a, v_a, q_b, k_b, v_b,
         gain_qa[None], gain_ka[None], gain_qb[None], gain_kb[None],
-        cos_a, sin_a, cos_b, sin_b,
+        freq_a, freq_b,
         w_out_a, w_out_b, gain_mid[None], w_gate, w_up, conv_gate, conv_up, w_down,
     )
 

time: 138 us -> 130 us (0.942)
  Pallas kernels: 131 us -> 125 us
  other arithmetic: 1.56 us -> 0.02 us
    pallas_call x1, Pallas kernels: 131 us -> 125 us  [on_device(): pl.pallas_call(functools.partial(kernel, n, tp_n), out_shape=jax.ShapeDty...]
where the time goes in v2:
time: 130 us
  Pallas kernels  125 us (96%)
  local copies, waits for them, and re-layouts  5.11 us (4%)
    pallas_call x1, Pallas kernels, on_device(): pl.pallas_call(functools.partial(kernel, n, tp_n), out_shape=jax.ShapeDty...  125 us
    unnamed x5, local copies, waits for them, and re-layouts  3.9 us

profile of v2, /device:TPU:0, one launch (start us, length us, event | category | flops | bytes accessed | tf_op | source)
XLA Modules:
  0.0 129.7 jit_solution(12662845667053300418)
XLA Ops:
  0.0 0.6 broadcast_in_dim_tile.7.frb_ref
  0.7 0.6 broadcast_in_dim_tile.6.fra_ref
  1.2 0.0 copy-start
  1.2 1.5 %copy.20.ka_hbm = bf16[256,64]{1,0:T(8,128)(2,1)} copy(bf16[256,64]{0,1:T(8,128)(2,1)} %param.21) | data formatting | bytes 65536 | tf_op args[2]
  2.7 0.0 copy-done
  2.7 0.7 copy.21.va_hbm
  3.5 124.6 %layer.1 = bf16[64,2048]{1,0:T(8,128)(2,1)} custom-call(bf16[64,2048]{1,0:T(8,128)(2,1)} %x_ref.1, bf16[256,256]{1,0:T(8,128)(2,1)} %qa_ref.1, bf16[256,64]{1,0:T(8,128)(2,1)} %copy.20.ka_hbm, bf16[256,64]{1,0:T(8,128)(2,1)} %copy.21.va_hbm, bf16[256,256]{1,0:T(8,128)(2,1)} %qb_ref.1, bf16[256,128]{1,0:T(8,128)(2,1)} %kb_ref.1, bf16[256,128]{1,0:T(8,128)(2,1)} %vb_ref.1, ...), custom_call_target="tpu_custom_call" | custom-call | tf_op jit(solution)/shard_map/layer/pallas_call | solution.py:545
  128.1 1.7 %copy.23 = bf16[64,2048]{1,0:T(8,128)(2,1)} copy(bf16[64,2048]{1,0:T(8,128)(2,1)} %layer.1) | data formatting | bytes 524288
  (4 shorter events, 0.0 us)
Async XLA Ops:
  1.2 1.5 %copy-start = (bf16[256,64]{0,1:T(8,128)(2,1)S(1)}, bf16[256,64]{0,1:T(8,128)(2,1)}, u32[]{:S(2)}) copy-start(bf16[256,64]{0,1:T(8,128)(2,1)} %param.22) | copy-start | bytes 98308
